TPU v7x, 256 devices: a whole 4x4x8 slice. The times are simulated.
256 devices in a mesh: ep: 64 (over z, y, core), tp: 4 (over x).
Axes of the slice: x: 4, y: 4, z: 8, core: 2. Of those that a mesh axis runs over, the one named last changes fastest.
Arguments:
- first_input: bfloat16 [32768, 2048], P('ep'), may hold values from -120 to 120
- first_gain: bfloat16 [2048], replicated, may hold values from 0.099609375 to 1.8984375
- pool_inward: bfloat16 [2048, 1024], P(None, 'tp'), may hold values from -0.125 to 0.125
- pool_mixing: bfloat16 [4, 256, 256], P('tp'), may hold values from -0.375 to 0.375
- pool_scale: bfloat16 [1024], P('tp'), may hold values from 0.099609375 to 1.8984375
- pool_outward: bfloat16 [1024, 2048], P('tp'), may hold values from -0.1875 to 0.1875
- second_input: bfloat16 [16384, 2048], P('ep'), may hold values from -120 to 120
- second_gain: bfloat16 [2048], replicated, may hold values from 0.099609375 to 1.8984375
- route_ids: int32 [16384, 2], P('ep'), may hold values from 0 to 31, all different within a row; in each aligned block of 256 rows (0 to 255, 256 to 511, ...) at most 18 rows name the same one
- route_logits: float32 [16384, 2], P('ep'), may hold values from -6 to 6
- expert_gate: bfloat16 [64, 2048, 2048], P('ep', None, 'tp'), may hold values from -0.125 to 0.125
- expert_up: bfloat16 [64, 2048, 2048], P('ep', None, 'tp'), may hold values from -0.125 to 0.125
- expert_down: bfloat16 [64, 2048, 2048], P('ep', 'tp'), may hold values from -0.09375 to 0.09375
Outputs:
- first_out: bfloat16 [32768, 2048], P('ep', 'tp')
- second_out: bfloat16 [16384, 2048], P('ep', 'tp')
Inputs may be any that keep to these rules, and one draw needn't show every extreme that they name: `route_ids`: each row names two different experts. In each aligned block of 256 rows (the rows of one index of ep) no expert is named by more than 18 rows, and in some blocks one expert is named by exactly 18 rows.
All inputs are finite; a program needn't handle non-finite values.
Results may differ from a plain program's by a relative error of at most 0.012.
Values may be sent and summed in bfloat16 or wider, within the bound.
No kernel may reach another device: no remote copies, remote signals or barrier semaphores. Data moves between devices by JAX's collectives and lax.ppermute only.
A program may use at most 64 MiB of HBM per device.

v0:
```python
import jax
import jax.numpy as jnp
from jax import lax
from jax.sharding import Mesh, PartitionSpec as P

epsilon = 1e-06


def from_behind(value, axis, steps):
    count = lax.axis_size(axis)
    leading, last = (max(0, -steps), min(count, count - steps))
    return lax.ppermute(value, axis, [(source, source + steps) for source in range(leading, last)])


def rms_scaled(values, weights):
    widened = values.astype(jnp.float32)
    inverse = lax.rsqrt(jnp.mean(widened * widened, axis=-1, keepdims=True) + epsilon)
    return (widened * inverse * weights.astype(jnp.float32)).astype(jnp.bfloat16)


def window_means(channels, length, offset):
    row_count = channels.shape[0] - 15
    summed = jnp.zeros((row_count, channels.shape[1]), jnp.float32)
    for lookback in range(16):
        summed = summed + jnp.where(
            lookback < length, channels[15 - lookback : 15 - lookback + row_count], 0.0
        )
    positions = offset + jnp.arange(row_count, dtype=jnp.int32)
    counts = jnp.minimum(positions + 1, length).astype(jnp.float32)
    return summed / counts[:, None]


def slot_positions(block_ids, expert_count, capacity):
    flattened = block_ids.reshape(-1)
    onehot = (flattened[:, None] == jnp.arange(expert_count, dtype=jnp.int32)[None, :]).astype(
        jnp.int32
    )
    running = jnp.cumsum(onehot, axis=0, dtype=jnp.int32) - 1
    slot_numbers = jnp.sum(onehot * running, axis=1)
    return flattened * capacity + slot_numbers


def expert_output(gate_sum, up_sum, down_rows):
    hidden = (jax.nn.silu(gate_sum) * up_sum).astype(jnp.bfloat16)
    return jnp.dot(hidden, down_rows, preferred_element_type=jnp.float32)


def local(
    first_input,
    first_gain,
    pool_inward,
    pool_mixing,
    pool_scale,
    pool_outward,
    second_input,
    second_gain,
    route_ids,
    route_logits,
    expert_gate,
    expert_up,
    expert_down,
):
    tensor_parts = lax.axis_size("tp")
    expert_count = lax.axis_size("z") * lax.axis_size("y")
    model_width = first_input.shape[1]
    quarter_width = model_width // tensor_parts
    swap = [(0, 1), (1, 0)]
    gate_other = lax.ppermute(expert_gate[0], "core", swap)
    up_other = lax.ppermute(expert_up[0], "core", swap)
    down_other = lax.ppermute(expert_down[0], "core", swap)
    normed_first = rms_scaled(first_input, first_gain)
    pooled_in = jnp.dot(normed_first, pool_inward, preferred_element_type=jnp.float32).astype(
        jnp.bfloat16
    )
    halo_rows = from_behind(pooled_in[-15:], ("z", "y", "core"), 1)
    extended = jnp.concatenate([halo_rows, pooled_in], axis=0).astype(jnp.float32)
    window = jnp.left_shift(jnp.int32(2), lax.axis_index("tp"))
    sequence_start = lax.axis_index(("z", "y", "core")) * first_input.shape[0]
    means = window_means(extended, window, sequence_start)
    mixed = (means - pooled_in.astype(jnp.float32)).astype(jnp.bfloat16)
    pooled = (
        jnp.dot(mixed, pool_mixing[0], preferred_element_type=jnp.float32)
        * pool_scale.astype(jnp.float32)
    ).astype(jnp.bfloat16)
    mixer_term = jnp.dot(pooled, pool_outward, preferred_element_type=jnp.float32)
    normed_second = rms_scaled(second_input, second_gain)
    row_count = second_input.shape[0]
    capacity = 2 * row_count * 9 // (8 * expert_count)
    positions = slot_positions(route_ids, expert_count, capacity)
    quarter = lax.dynamic_slice_in_dim(
        normed_second, lax.axis_index("tp") * quarter_width, quarter_width, 1
    )
    repeated = jnp.repeat(quarter, 2, axis=0)
    buffer = (
        jnp.zeros((expert_count * capacity, quarter_width), jnp.bfloat16)
        .at[positions]
        .set(repeated)
        .reshape(expert_count, capacity, quarter_width)
    )
    arrived = lax.all_to_all(buffer, ("z", "y"), split_axis=0, concat_axis=0, tiled=True)
    flattened = arrived.reshape(-1, quarter_width)
    portion = lax.all_gather(flattened, "tp", axis=1, tiled=True)
    flat_term = expert_output(
        jnp.dot(portion, expert_gate[0], preferred_element_type=jnp.float32),
        jnp.dot(portion, expert_up[0], preferred_element_type=jnp.float32),
        expert_down[0],
    ) + expert_output(
        jnp.dot(portion, gate_other, preferred_element_type=jnp.float32),
        jnp.dot(portion, up_other, preferred_element_type=jnp.float32),
        down_other,
    )
    first_out = lax.psum_scatter(
        mixer_term.astype(jnp.bfloat16), "tp", scatter_dimension=1, tiled=True
    )
    expert_summed = lax.psum_scatter(
        flat_term.astype(jnp.bfloat16), "tp", scatter_dimension=1, tiled=True
    )
    half_out = expert_summed.reshape(expert_count, capacity, quarter_width)
    returned = lax.all_to_all(half_out, ("z", "y"), split_axis=0, concat_axis=0, tiled=True)
    route_out = returned.reshape(-1, quarter_width).astype(jnp.float32)
    picked = route_out[positions].reshape(row_count, 2, quarter_width)
    shares = jax.nn.sigmoid(route_logits - route_logits[:, ::-1])
    second_out = jnp.sum(picked * shares[:, :, None], axis=1).astype(jnp.bfloat16)
    return (first_out, second_out)


def solution(mesh):
    split_mesh = Mesh(mesh.devices.reshape(8, 4, 2, 4), ("z", "y", "core", "tp"))
    ep = ("z", "y", "core")
    placed = (
        P(ep, None),
        P(),
        P(None, "tp"),
        P("tp", None, None),
        P("tp"),
        P("tp", None),
        P(ep, None),
        P(),
        P(ep, None),
        P(ep, None),
        P(ep, None, "tp"),
        P(ep, None, "tp"),
        P(ep, "tp", None),
    )
    return jax.shard_map(
        local,
        mesh=split_mesh,
        in_specs=placed,
        out_specs=(P(ep, "tp"), P(ep, "tp")),
        check_vma=False,
    )
```

profile of v0, /device:TPU:8, one launch (start us, length us, event | category | flops | bytes accessed | tf_op | source)
XLA Modules:
  0.0 189.3 jit_solution(17867324479856150440)
XLA Ops:
  7.3 3.0 %convert_element_type.81 = f32[256,2048]{1,0:T(8,128)} convert(bf16[256,2048]{1,0:T(8,128)(2,1)} %param.19) | non-fusion elementwise | flops 524288 | bytes 3145728 | tf_op jit(solution)/shard_map/convert_element_type | solution.py:16
  11.1 1.2 fusion.16
  12.7 1.2 reduce-window.6
  14.6 2.6 %scatter_custom_fusion = bf16[576,512]{1,0:T(8,128)(2,1)S(1)} fusion(s32[512]{0:T(512)S(1)} %bitcast.40, bf16[512,512]{1,0:T(8,128)(2,1)S(1)} %reshape.116, bf16[]{:T(256)} %constant.77.clone.1), kind=kCustom, calls=%fused_computation.60 | custom fusion | bytes 589826 | tf_op jit(solution)/shard_map/scatter | solution.py:97
  17.3 33.9 %all_to_all.10 = bf16[32,18,512]{2,1,0:T(8,128)(2,1)S(1)} all-to-all(bf16[32,18,512]{2,1,0:T(8,128)(2,1)S(1)} %reshape.99), channel_id=1, replica_groups=mesh['z'=8,'y'=4,'core'=2,'tp'=4] {'z','y'}, dimensions={0} | all-to-all | bytes 1179648 | tf_op jit(solution)/shard_map/all_to_all | solution.py:100
  51.3 1.0 reshape.100
  53.0 31.6 %all-gather.2.cloned.1.call-done = bf16[576,2048]{1,0:T(8,128)(2,1)} async-done(((bf16[576,512]{1,0:T(8,128)(2,1)}), bf16[576,2048]{1,0:T(8,128)(2,1)}) %all-gather.2.cloned.1.call-update) | async-done | bytes 2359312 | tf_op jit(solution)/shard_map/all_gather | solution.py:102
  84.6 4.9 %fusion.80 = f32[576,512]{1,0:T(8,128)} fusion(bf16[576,2048]{1,0:T(8,128)(2,1)} %all-gather.2.cloned.1.call-done, bf16[1,2048,512]{2,1,0:T(8,128)(2,1)} %param.23), kind=kOutput, calls=%fused_computation.98 | convolution fusion | flops 1207959552 | bytes 5636096 | tf_op jit(solution)/shard_map/dot_general | solution.py:104
  89.5 4.0 %fusion.88 = f32[576,512]{1,0:T(8,128)} fusion(bf16[576,2048]{1,0:T(8,128)(2,1)S(1)} %copy-done.7, bf16[2048,512]{1,0:T(8,128)(2,1)} %collective-permute-done.1), kind=kOutput, calls=%fused_computation.104 | convolution fusion | flops 1207959552 | bytes 5636096 | tf_op jit(solution)/shard_map/dot_general | solution.py:108
  93.5 7.4 %fusion.12 = f32[576,2048]{1,0:T(8,128)} fusion(bf16[576,2048]{1,0:T(8,128)(2,1)S(1)} %copy-done.7, f32[576,512]{1,0:T(8,128)} %fusion.80, bf16[1,512,2048]{2,1,0:T(8,128)(2,1)} %param.25, bf16[1,2048,512]{2,1,0:T(8,128)(2,1)} %param.24), kind=kOutput, calls=%fused_computation.20 | convolution fusion | flops 2417688576 | bytes 12451840 | tf_op jit(solution)/shard_map/dot_general | solution.py:45
  100.9 8.1 %add_convert_fusion = bf16[576,2048]{1,0:T(8,128)(2,1)} fusion(f32[576,2048]{1,0:T(8,128)} %fusion.12, bf16[512,2048]{1,0:T(8,128)(2,1)} %collective-permute-done.3, f32[576,512]{1,0:T(8,128)} %fusion.88, bf16[576,2048]{1,0:T(8,128)(2,1)S(1)} %copy-done.7, bf16[2048,512]{1,0:T(8,128)(2,1)} %collective-permute-done.2), kind=kOutput, calls=%fused_computation.4 | convolution fusion | flops 2420047872 | bytes 14811136 | tf_op jit(solution)/shard_map/dot_general | solution.py:45
  109.1 0.6 copy-done.5
  109.7 0.9 copy-done.2
  111.2 0.8 fusion.8
  112.0 1.9 %collective-permute-start = (bf16[15,256]{1,0:T(8,128)(2,1)S(1)}, bf16[15,256]{1,0:T(8,128)(2,1)S(1)}, u32[]{:S(2)}, u32[]{:S(2)}) collective-permute-start(bf16[15,256]{1,0:T(8,128)(2,1)S(1)} %slice.78), channel_id=1, source_target_pairs={{0,4},{4,8},{8,12},{12,16},{16,20},{20,24},{24,28},{28,32},{32,36}... | collective-permute-start | bytes 23048 | tf_op jit(solution)/shard_map/ppermute | solution.py:12
  114.0 3.0 %collective-permute-done = bf16[15,256]{1,0:T(8,128)(2,1)S(1)} collective-permute-done((bf16[15,256]{1,0:T(8,128)(2,1)S(1)}, bf16[15,256]{1,0:T(8,128)(2,1)S(1)}, u32[]{:S(2)}, u32[]{:S(2)}) %collective-permute-start) | collective-permute-done | bytes 7712 | tf_op jit(solution)/shard_map/ppermute | solution.py:12
  117.0 3.5 %convolution_convert_fusion = bf16[512,2048]{1,0:T(8,128)(2,1)} fusion(bf16[256,2048]{1,0:T(8,128)(2,1)S(1)} %copy-done, f32[256]{0:T(256)S(1)} %convert_element_type.77, bf16[512,256]{1,0:T(8,128)(2,1)S(1)} %fusion.8, f32[527,256]{1,0:T(8,128)S(1)} %maximum_convert_fusion, f32[512]{0:T(512)S(1)} %minimum_convert_fusion, pred[]{:T(512)S(6)} %gt.63, ...), kind=kOutput, calls=%fused_computation.8 | convolution fusion | flops 609878016 | bytes 11930640 | tf_op jit(solution)/shard_map/dot_general | solution.py:85
  120.5 23.2 %reduce-scatter.5.cloned.1.call-done = bf16[576,512]{1,0:T(8,128)(2,1)} async-done(((bf16[576,2048]{1,0:T(8,128)(2,1)}), bf16[576,512]{1,0:T(8,128)(2,1)}) %reduce-scatter.5.cloned.1.call-update) | async-done | bytes 589840 | tf_op jit(solution)/shard_map/reduce_scatter | solution.py:115
  143.7 2.1 %reshape.101 = bf16[32,18,512]{2,1,0:T(8,128)(2,1)} reshape(bf16[576,512]{1,0:T(8,128)(2,1)} %reduce-scatter.5.cloned.1.call-done) | data formatting | bytes 1179648 | tf_op jit(solution)/shard_map/reshape | solution.py:118
  145.8 10.2 %all-to-all-start.1 = ((bf16[32,18,512]{2,1,0:T(8,128)(2,1)}), bf16[32,18,512]{2,1,0:T(8,128)(2,1)S(1)}, u32[]{:S(2)}, u32[]{:S(2)}) async-start(bf16[32,18,512]{2,1,0:T(8,128)(2,1)} %reshape.101), calls=%async_computation.3 | async-start | bytes 1572864 | tf_op jit(solution)/shard_map/all_to_all | solution.py:119
  156.3 22.1 %all-to-all-done.1 = bf16[32,18,512]{2,1,0:T(8,128)(2,1)S(1)} async-done(((bf16[32,18,512]{2,1,0:T(8,128)(2,1)}), bf16[32,18,512]{2,1,0:T(8,128)(2,1)S(1)}, u32[]{:S(2)}, u32[]{:S(2)}) %all-to-all-start.1) | async-done | bytes 589856 | tf_op jit(solution)/shard_map/all_to_all | solution.py:119
  178.5 1.6 gather_fusion
  180.1 0.6 reshape.102
  180.8 2.1 %multiply_reduce_fusion.1 = bf16[256,512]{1,0:T(8,128)(2,1)} fusion(f32[256,2,512]{2,1,0:T(2,128)S(1)} %reshape.102, f32[256,2]{1,0:T(8,128)S(1)} %copy.20), kind=kLoop, calls=%fused_computation.19 | loop fusion | flops 393216 | bytes 1312768 | tf_op jit(solution)/shard_map/reduce_sum | solution.py:123
  (63 shorter events, 4.0 us)
Async XLA Ops:
  7.2 109.8 %copy-start = (bf16[256,2048]{1,0:T(8,128)(2,1)S(1)}, bf16[256,2048]{1,0:T(8,128)(2,1)}, u32[]{:S(2)}) copy-start(bf16[256,2048]{1,0:T(8,128)(2,1)} %param.18) | copy-start | bytes 3145732
  7.2 3.0 %copy-start.1 = (bf16[256,2048]{1,0:T(8,128)(2,1)S(1)}, bf16[256,2048]{1,0:T(8,128)(2,1)}, u32[]{:S(2)}) copy-start(bf16[256,2048]{1,0:T(8,128)(2,1)} %param.19) | copy-start | bytes 3145732
  7.2 77.5 %all-gather.2.cloned.1.call-start = ((), (), s32[]{:S(2)}) async-start(), calls=%async_computation.5 | async-start | bytes 2949120 | tf_op jit(solution)/shard_map/all_gather | solution.py:102
  7.2 3.3 %copy-start.3 = (s32[256,2]{0,1:T(2,128)S(1)}, s32[256,2]{0,1:T(2,128)}, u32[]{:S(2)}) copy-start(s32[256,2]{0,1:T(2,128)} %param.21) | copy-start | bytes 6148
  7.2 3.7 %copy-start.6 = (bf16[2048]{0:T(1024)(128)(2,1)S(1)}, bf16[2048]{0:T(1024)(128)(2,1)}, u32[]{:S(2)}) copy-start(bf16[2048]{0:T(1024)(128)(2,1)} %param.20) | copy-start | bytes 12292
  52.3 91.4 %reduce-scatter.5.cloned.1.call-start = ((), (), s32[]{:S(2)}) async-start(), calls=%async_computation.6 | async-start | bytes 2949120 | tf_op jit(solution)/shard_map/reduce_scatter | solution.py:115
  52.3 37.2 %collective-permute-start.1 = (bf16[2048,512]{1,0:T(8,128)(2,1)}, bf16[2048,512]{1,0:T(8,128)(2,1)}, u32[]{:S(2)}, u32[]{:S(2)}) collective-permute-start(bf16[2048,512]{1,0:T(8,128)(2,1)} %bitcast.43), channel_id=1, source_target_pairs={{0,4},{4,0},{1,5},{5,1},{2,6},{6,2},{3,7},{7,3},{8,12},{12,8},{9,1... | collective-permute-start | bytes 6291464 | tf_op jit(solution)/shard_map/ppermute | solution.py:68
  52.4 48.5 %collective-permute-start.2 = (bf16[2048,512]{1,0:T(8,128)(2,1)}, bf16[2048,512]{1,0:T(8,128)(2,1)}, u32[]{:S(2)}, u32[]{:S(2)}) collective-permute-start(bf16[2048,512]{1,0:T(8,128)(2,1)} %bitcast.44), channel_id=1, source_target_pairs={{0,4},{4,0},{1,5},{5,1},{2,6},{6,2},{3,7},{7,3},{8,12},{12,8},{9,1... | collective-permute-start | bytes 6291464 | tf_op jit(solution)/shard_map/ppermute | solution.py:69
  52.9 48.0 %collective-permute-start.3 = (bf16[512,2048]{1,0:T(8,128)(2,1)}, bf16[512,2048]{1,0:T(8,128)(2,1)}, u32[]{:S(2)}, u32[]{:S(2)}) collective-permute-start(bf16[512,2048]{1,0:T(8,128)(2,1)} %bitcast.45), channel_id=1, source_target_pairs={{0,4},{4,0},{1,5},{5,1},{2,6},{6,2},{3,7},{7,3},{8,12},{12,8},{9,1... | collective-permute-start | bytes 6291464 | tf_op jit(solution)/shard_map/ppermute | solution.py:70
  84.6 4.9 %copy-start.7 = (bf16[576,2048]{1,0:T(8,128)(2,1)S(1)}, bf16[576,2048]{1,0:T(8,128)(2,1)}, u32[]{:S(2)}) copy-start(bf16[576,2048]{1,0:T(8,128)(2,1)} %all-gather.2.cloned.1.call-done) | copy-start | bytes 7077892
  109.0 0.7 copy-start.5
  109.0 1.6 copy-start.2
  109.1 73.8 %reduce-scatter.3.cloned.1.call-start = ((), (), s32[]{:S(2)}) async-start(), calls=%async_computation.4 | async-start | bytes 2621440 | tf_op jit(solution)/shard_map/reduce_scatter | solution.py:112
  109.7 1.4 copy-start.8
  111.1 2.8 %copy-start.10 = (bf16[256]{0:T(256)(128)(2,1)S(1)}, bf16[256]{0:T(256)(128)(2,1)}, u32[]{:S(2)}) copy-start(bf16[256]{0:T(256)(128)(2,1)} %param.17) | copy-start | bytes 1540
  111.2 5.9 %copy-start.9 = (bf16[1,256,256]{2,1,0:T(8,128)(2,1)S(1)}, bf16[1,256,256]{2,1,0:T(8,128)(2,1)}, u32[]{:S(2)}) copy-start(bf16[1,256,256]{2,1,0:T(8,128)(2,1)} %param.16) | copy-start | bytes 393220
  112.0 5.0 %collective-permute-start = (bf16[15,256]{1,0:T(8,128)(2,1)S(1)}, bf16[15,256]{1,0:T(8,128)(2,1)S(1)}, u32[]{:S(2)}, u32[]{:S(2)}) collective-permute-start(bf16[15,256]{1,0:T(8,128)(2,1)S(1)} %slice.78), channel_id=1, source_target_pairs={{0,4},{4,8},{8,12},{12,16},{16,20},{20,24},{24,28},{28,32},{32,36}... | collective-permute-start | bytes 23048 | tf_op jit(solution)/shard_map/ppermute | solution.py:12
  120.5 35.5 %copy-start.4 = (f32[256,2]{0,1:T(2,128)S(1)}, f32[256,2]{0,1:T(2,128)}, u32[]{:S(2)}) copy-start(f32[256,2]{0,1:T(2,128)} %param.22) | copy-start | bytes 6148
  145.8 32.5 %all-to-all-start.1 = ((bf16[32,18,512]{2,1,0:T(8,128)(2,1)}), bf16[32,18,512]{2,1,0:T(8,128)(2,1)S(1)}, u32[]{:S(2)}, u32[]{:S(2)}) async-start(bf16[32,18,512]{2,1,0:T(8,128)(2,1)} %reshape.101), calls=%async_computation.3 | async-start | bytes 1572864 | tf_op jit(solution)/shard_map/all_to_all | solution.py:119
Sparse Core Ops, SparseCore 0:
  52.4 32.2 all-gather.1
  109.2 34.4 reduce-scatter.4
  146.8 31.9 reduce-scatter.2
where the time goes:
time: 190 us; the launch traced here: 189 us
  waiting for transfers between devices  79.9 us (42%)
  blocking collectives  33.9 us (18%)
  matrix products  28.7 us (15%)
  between operations  14.1 us (7%)
  starting transfers between devices  12.9 us (7%)
  local copies, waits for them, and re-layouts  11.5 us (6%)
  other arithmetic  8.35 us (4%)
    all_to_all x1, blocking collectives, local(): lax.all_to_all(buffer, ('z', 'y'), split_axis=0, concat_axis=0, tiled=True)  33.9 us
    all_gather x1, waiting for transfers between devices, local(): portion = lax.all_gather(flattened, 'tp', axis=1, tiled=True)  31.6 us
    reduce_scatter x1, waiting for transfers between devices, local(): lax.psum_scatter(flat_term.astype(jnp.bfloat16), 'tp', scatter_dimension=...  23.2 us
    all_to_all x1, waiting for transfers between devices, local(): lax.all_to_all(half_out, ('z', 'y'), split_axis=0, concat_axis=0, tiled=T...  22.1 us
    dot_general x2, matrix products, expert_output(): return jnp.dot(hidden, down_rows, preferred_element_type=jnp.float32)  15.5 us
    all_to_all x1, starting transfers between devices, local(): lax.all_to_all(half_out, ('z', 'y'), split_axis=0, concat_axis=0, tiled=T...  10.2 us
    dot_general x1, matrix products, local(): jnp.dot(portion, expert_gate[0], preferred_element_type=jnp.float32)  4.89 us
    dot_general x1, matrix products, local(): jnp.dot(portion, gate_other, preferred_element_type=jnp.float32)  3.97 us
  transfers between devices with their start and end apart: 8, of which 4 were waited for; matrix products, arithmetic and copies ran while one was open for 15% of the time, Pallas kernels for 0%

commit v1 on v0

--- a/solution.py
+++ b/solution.py
@@ -60,6 +60,13 @@
     expert_up,
     expert_down,
 ):
+
+    def place_the_sample(buf, axis_id):
+        kept_arr = lax.axis_size(axis_id)
+        finding = jnp.stack([buf] * kept_arr)
+        ready = lax.all_to_all(finding, axis_id, 0, 0)
+        return jnp.concatenate(ready, 1)
+
     tensor_parts = lax.axis_size("tp")
     expert_count = lax.axis_size("z") * lax.axis_size("y")
     model_width = first_input.shape[1]
@@ -99,7 +106,7 @@
     )
     arrived = lax.all_to_all(buffer, ("z", "y"), split_axis=0, concat_axis=0, tiled=True)
     flattened = arrived.reshape(-1, quarter_width)
-    portion = lax.all_gather(flattened, "tp", axis=1, tiled=True)
+    portion = place_the_sample(flattened, "tp")
     flat_term = expert_output(
         jnp.dot(portion, expert_gate[0], preferred_element_type=jnp.float32),
         jnp.dot(portion, expert_up[0], preferred_element_type=jnp.float32),

time: 190 us -> 184 us (0.968)
  waiting for transfers between devices: 79.9 us -> 70.4 us
  starting transfers between devices: 12.9 us -> 17 us
  local copies, waits for them, and re-layouts: 11.5 us -> 14.7 us
  other arithmetic: 8.35 us -> 5.95 us
    all_gather x1 -> x0, waiting for transfers between devices: 31.6 us -> none  [local(): portion = lax.all_gather(flattened, 'tp', axis=1, tiled=True)]
    all_to_all x0 -> x1, waiting for transfers between devices: none -> 26.9 us  [place_the_sample(): ready = lax.all_to_all(finding, axis_id, 0, 0)]
    reduce_scatter x1, waiting for transfers between devices: 23.2 us -> 18.4 us  [local(): lax.psum_scatter(flat_term.astype(jnp.bfloat16), 'tp', scatter_dimension=...]
    all_to_all x0 -> x1, starting transfers between devices: none -> 4.29 us  [place_the_sample(): ready = lax.all_to_all(finding, axis_id, 0, 0)]
    dot_general x1, matrix products: 4.89 us -> 2.47 us  [local(): jnp.dot(portion, expert_gate[0], preferred_element_type=jnp.float32)]
    unnamed x23 -> x27, local copies, waits for them, and re-layouts: 1.71 us -> 3.81 us
where the time goes in v1:
time: 184 us
  waiting for transfers between devices  70.4 us (38%)
  blocking collectives  33.9 us (18%)
  matrix products  27.1 us (15%)
  starting transfers between devices  17 us (9%)
  local copies, waits for them, and re-layouts  14.7 us (8%)
  between operations  14.4 us (8%)
  other arithmetic  5.95 us (3%)
    all_to_all x1, blocking collectives, local(): lax.all_to_all(buffer, ('z', 'y'), split_axis=0, concat_axis=0, tiled=True)  33.9 us
    all_to_all x1, waiting for transfers between devices, place_the_sample(): ready = lax.all_to_all(finding, axis_id, 0, 0)  26.9 us
    all_to_all x1, waiting for transfers between devices, local(): lax.all_to_all(half_out, ('z', 'y'), split_axis=0, concat_axis=0, tiled=T...  22.1 us
    reduce_scatter x1, waiting for transfers between devices, local(): lax.psum_scatter(flat_term.astype(jnp.bfloat16), 'tp', scatter_dimension=...  18.4 us
    dot_general x2, matrix products, expert_output(): return jnp.dot(hidden, down_rows, preferred_element_type=jnp.float32)  16.4 us
    all_to_all x1, starting transfers between devices, local(): lax.all_to_all(half_out, ('z', 'y'), split_axis=0, concat_axis=0, tiled=T...  10.2 us
    all_to_all x1, starting transfers between devices, place_the_sample(): ready = lax.all_to_all(finding, axis_id, 0, 0)  4.29 us
    dot_general x1, matrix products, local(): jnp.dot(portion, gate_other, preferred_element_type=jnp.float32)  3.99 us
  transfers between devices with their start and end apart: 8, of which 4 were waited for; matrix products, arithmetic and copies ran while one was open for 15% of the time, Pallas kernels for 0%

profile of v1, /device:TPU:8, one launch (start us, length us, event | category | flops | bytes accessed | tf_op | source)
XLA Modules:
  0.0 183.6 jit_solution(6292548652725823668)
XLA Ops:
  7.2 1.6 convert_element_type.81
  10.3 1.2 reduce-window.6
  12.1 2.6 %scatter_custom_fusion = bf16[576,512]{1,0:T(8,128)(2,1)S(1)} fusion(s32[512]{0:T(512)S(1)} %bitcast.48, bf16[512,512]{1,0:T(8,128)(2,1)S(1)} %reshape.122, bf16[]{:T(256)} %constant.77.clone.1), kind=kCustom, calls=%fused_computation.60 | custom fusion | bytes 589826 | tf_op jit(solution)/shard_map/scatter | solution.py:104
  14.9 33.9 %all_to_all.15 = bf16[32,18,512]{2,1,0:T(8,128)(2,1)S(1)} all-to-all(bf16[32,18,512]{2,1,0:T(8,128)(2,1)S(1)} %reshape.104), channel_id=1, replica_groups=mesh['z'=8,'y'=4,'core'=2,'tp'=4] {'z','y'}, dimensions={0} | all-to-all | bytes 1179648 | tf_op jit(solution)/shard_map/all_to_all | solution.py:107
  49.0 1.6 stack.3
  50.6 4.3 %all-to-all-start.1 = ((bf16[4,576,512]{2,1,0:T(8,128)(2,1)}), bf16[4,576,512]{2,1,0:T(8,128)(2,1)S(1)}, u32[]{:S(2)}, u32[]{:S(2)}) async-start(bf16[4,576,512]{2,1,0:T(8,128)(2,1)} %stack.3), calls=%async_computation.2 | async-start | bytes 4718592 | tf_op jit(solution)/shard_map/all_to_all | solution.py:67
  55.5 26.9 %all-to-all-done.1 = bf16[4,576,512]{2,1,0:T(8,128)(2,1)S(1)} async-done(((bf16[4,576,512]{2,1,0:T(8,128)(2,1)}), bf16[4,576,512]{2,1,0:T(8,128)(2,1)S(1)}, u32[]{:S(2)}, u32[]{:S(2)}) %all-to-all-start.1) | async-done | bytes 2359328 | tf_op jit(solution)/shard_map/all_to_all | solution.py:67
  82.7 2.1 %copy-done.9 = bf16[1,2048,512]{2,1,0:T(8,128)(2,1)S(1)} copy-done((bf16[1,2048,512]{2,1,0:T(8,128)(2,1)S(1)}, bf16[1,2048,512]{2,1,0:T(8,128)(2,1)}, u32[]{:S(2)}) %copy-start.9) | copy-done | bytes 2097176
  84.8 2.5 %fusion.80 = f32[576,512]{1,0:T(8,128)} fusion(bf16[576,2048]{1,0:T(8,128)(2,1)S(1)} %bitcast.44, bf16[1,2048,512]{2,1,0:T(8,128)(2,1)S(1)} %copy-done.9), kind=kOutput, calls=%fused_computation.98 | convolution fusion | flops 1207959552 | bytes 5636096 | tf_op jit(solution)/shard_map/dot_general | solution.py:111
  87.3 4.0 %fusion.88 = f32[576,512]{1,0:T(8,128)} fusion(bf16[576,2048]{1,0:T(8,128)(2,1)S(1)} %bitcast.45, bf16[2048,512]{1,0:T(8,128)(2,1)} %collective-permute-done.1), kind=kOutput, calls=%fused_computation.104 | convolution fusion | flops 1207959552 | bytes 5636096 | tf_op jit(solution)/shard_map/dot_general | solution.py:115
  91.3 8.3 %fusion.12 = f32[576,2048]{1,0:T(8,128)} fusion(bf16[576,2048]{1,0:T(8,128)(2,1)} %bitcast.46, f32[576,512]{1,0:T(8,128)} %fusion.80, bf16[1,512,2048]{2,1,0:T(8,128)(2,1)} %param.25, bf16[1,2048,512]{2,1,0:T(8,128)(2,1)} %param.24), kind=kOutput, calls=%fused_computation.20 | convolution fusion | flops 2417688576 | bytes 12451840 | tf_op jit(solution)/shard_map/dot_general | solution.py:45
  99.6 8.1 %add_convert_fusion = bf16[576,2048]{1,0:T(8,128)(2,1)} fusion(f32[576,2048]{1,0:T(8,128)} %fusion.12, bf16[512,2048]{1,0:T(8,128)(2,1)} %collective-permute-done.3, f32[576,512]{1,0:T(8,128)} %fusion.88, bf16[576,2048]{1,0:T(8,128)(2,1)S(1)} %bitcast.47, bf16[2048,512]{1,0:T(8,128)(2,1)} %collective-permute-done.2), kind=kOutput, calls=%fused_computation.4 | convolution fusion | flops 2420047872 | bytes 14811136 | tf_op jit(solution)/shard_map/dot_general | solution.py:45
  108.4 0.9 copy-done.4
  109.8 0.8 fusion.8
  110.6 1.9 %collective-permute-start = (bf16[15,256]{1,0:T(8,128)(2,1)S(1)}, bf16[15,256]{1,0:T(8,128)(2,1)S(1)}, u32[]{:S(2)}, u32[]{:S(2)}) collective-permute-start(bf16[15,256]{1,0:T(8,128)(2,1)S(1)} %slice.78), channel_id=1, source_target_pairs={{0,4},{4,8},{8,12},{12,16},{16,20},{20,24},{24,28},{28,32},{32,36}... | collective-permute-start | bytes 23048 | tf_op jit(solution)/shard_map/ppermute | solution.py:12
  112.6 3.0 %collective-permute-done = bf16[15,256]{1,0:T(8,128)(2,1)S(1)} collective-permute-done((bf16[15,256]{1,0:T(8,128)(2,1)S(1)}, bf16[15,256]{1,0:T(8,128)(2,1)S(1)}, u32[]{:S(2)}, u32[]{:S(2)}) %collective-permute-start) | collective-permute-done | bytes 7712 | tf_op jit(solution)/shard_map/ppermute | solution.py:12
  115.7 3.5 %convolution_convert_fusion = bf16[512,2048]{1,0:T(8,128)(2,1)} fusion(bf16[256,2048]{1,0:T(8,128)(2,1)S(1)} %copy-done, f32[256]{0:T(256)S(1)} %convert_element_type.77, bf16[512,256]{1,0:T(8,128)(2,1)S(1)} %fusion.8, f32[527,256]{1,0:T(8,128)S(1)} %maximum_convert_fusion, f32[512]{0:T(512)S(1)} %minimum_convert_fusion, pred[]{:T(512)S(6)} %gt.63, ...), kind=kOutput, calls=%fused_computation.8 | convolution fusion | flops 609878016 | bytes 11930640 | tf_op jit(solution)/shard_map/dot_general | solution.py:92
  119.2 18.4 %reduce-scatter.5.cloned.1.call-done = bf16[576,512]{1,0:T(8,128)(2,1)} async-done(((bf16[576,2048]{1,0:T(8,128)(2,1)}), bf16[576,512]{1,0:T(8,128)(2,1)}) %reduce-scatter.5.cloned.1.call-update) | async-done | bytes 589840 | tf_op jit(solution)/shard_map/reduce_scatter | solution.py:122
  137.6 2.1 %reshape.107 = bf16[32,18,512]{2,1,0:T(8,128)(2,1)} reshape(bf16[576,512]{1,0:T(8,128)(2,1)} %reduce-scatter.5.cloned.1.call-done) | data formatting | bytes 1179648 | tf_op jit(solution)/shard_map/reshape | solution.py:125
  139.7 10.2 %all-to-all-start.2 = ((bf16[32,18,512]{2,1,0:T(8,128)(2,1)}), bf16[32,18,512]{2,1,0:T(8,128)(2,1)S(1)}, u32[]{:S(2)}, u32[]{:S(2)}) async-start(bf16[32,18,512]{2,1,0:T(8,128)(2,1)} %reshape.107), calls=%async_computation.4 | async-start | bytes 1572864 | tf_op jit(solution)/shard_map/all_to_all | solution.py:126
  150.1 22.1 %all-to-all-done.2 = bf16[32,18,512]{2,1,0:T(8,128)(2,1)S(1)} async-done(((bf16[32,18,512]{2,1,0:T(8,128)(2,1)}), bf16[32,18,512]{2,1,0:T(8,128)(2,1)S(1)}, u32[]{:S(2)}, u32[]{:S(2)}) %all-to-all-start.2) | async-done | bytes 589856 | tf_op jit(solution)/shard_map/all_to_all | solution.py:126
  172.4 1.6 gather_fusion
  174.0 0.6 reshape.108
  174.7 2.1 %multiply_reduce_fusion.1 = bf16[256,512]{1,0:T(8,128)(2,1)} fusion(f32[256,2,512]{2,1,0:T(2,128)S(1)} %reshape.108, f32[256,2]{1,0:T(8,128)S(1)} %copy.26), kind=kLoop, calls=%fused_computation.19 | loop fusion | flops 393216 | bytes 1312768 | tf_op jit(solution)/shard_map/reduce_sum | solution.py:130
  (68 shorter events, 5.0 us)
Async XLA Ops:
  7.2 108.5 %copy-start = (bf16[256,2048]{1,0:T(8,128)(2,1)S(1)}, bf16[256,2048]{1,0:T(8,128)(2,1)}, u32[]{:S(2)}) copy-start(bf16[256,2048]{1,0:T(8,128)(2,1)} %param.18) | copy-start | bytes 3145732
  7.2 1.6 copy-start.1
  7.2 1.9 %copy-start.5 = (s32[256,2]{0,1:T(2,128)S(1)}, s32[256,2]{0,1:T(2,128)}, u32[]{:S(2)}) copy-start(s32[256,2]{0,1:T(2,128)} %param.21) | copy-start | bytes 6148
  7.2 2.4 %copy-start.8 = (bf16[2048]{0:T(1024)(128)(2,1)S(1)}, bf16[2048]{0:T(1024)(128)(2,1)}, u32[]{:S(2)}) copy-start(bf16[2048]{0:T(1024)(128)(2,1)} %param.20) | copy-start | bytes 12292
  50.6 31.8 %all-to-all-start.1 = ((bf16[4,576,512]{2,1,0:T(8,128)(2,1)}), bf16[4,576,512]{2,1,0:T(8,128)(2,1)S(1)}, u32[]{:S(2)}, u32[]{:S(2)}) async-start(bf16[4,576,512]{2,1,0:T(8,128)(2,1)} %stack.3), calls=%async_computation.2 | async-start | bytes 4718592 | tf_op jit(solution)/shard_map/all_to_all | solution.py:67
  54.9 82.7 %reduce-scatter.5.cloned.1.call-start = ((), (), s32[]{:S(2)}) async-start(), calls=%async_computation.6 | async-start | bytes 2949120 | tf_op jit(solution)/shard_map/reduce_scatter | solution.py:122
  54.9 32.4 %collective-permute-start.1 = (bf16[2048,512]{1,0:T(8,128)(2,1)}, bf16[2048,512]{1,0:T(8,128)(2,1)}, u32[]{:S(2)}, u32[]{:S(2)}) collective-permute-start(bf16[2048,512]{1,0:T(8,128)(2,1)} %bitcast.51), channel_id=1, source_target_pairs={{0,4},{4,0},{1,5},{5,1},{2,6},{6,2},{3,7},{7,3},{8,12},{12,8},{9,1... | collective-permute-start | bytes 6291464 | tf_op jit(solution)/shard_map/ppermute | solution.py:75
  54.9 44.6 %collective-permute-start.2 = (bf16[2048,512]{1,0:T(8,128)(2,1)}, bf16[2048,512]{1,0:T(8,128)(2,1)}, u32[]{:S(2)}, u32[]{:S(2)}) collective-permute-start(bf16[2048,512]{1,0:T(8,128)(2,1)} %bitcast.52), channel_id=1, source_target_pairs={{0,4},{4,0},{1,5},{5,1},{2,6},{6,2},{3,7},{7,3},{8,12},{12,8},{9,1... | collective-permute-start | bytes 6291464 | tf_op jit(solution)/shard_map/ppermute | solution.py:76
  55.4 44.1 %collective-permute-start.3 = (bf16[512,2048]{1,0:T(8,128)(2,1)}, bf16[512,2048]{1,0:T(8,128)(2,1)}, u32[]{:S(2)}, u32[]{:S(2)}) collective-permute-start(bf16[512,2048]{1,0:T(8,128)(2,1)} %bitcast.53), channel_id=1, source_target_pairs={{0,4},{4,0},{1,5},{5,1},{2,6},{6,2},{3,7},{7,3},{8,12},{12,8},{9,1... | collective-permute-start | bytes 6291464 | tf_op jit(solution)/shard_map/ppermute | solution.py:77
  82.4 2.4 %copy-start.9 = (bf16[1,2048,512]{2,1,0:T(8,128)(2,1)S(1)}, bf16[1,2048,512]{2,1,0:T(8,128)(2,1)}, u32[]{:S(2)}) copy-start(bf16[1,2048,512]{2,1,0:T(8,128)(2,1)} %param.23) | copy-start | bytes 6291460
  82.7 4.6 %copy-start.2 = (bf16[4,72,8,512]{3,2,0,1:T(8,128)(2,1)}, bf16[4,72,8,512]{3,2,0,1:T(8,128)(2,1)S(1)}, u32[]{:S(2)}) copy-start(bf16[4,72,8,512]{3,2,0,1:T(8,128)(2,1)S(1)} %copy.28) | copy-start | bytes 7077892
  91.3 8.3 %copy-start.3 = (bf16[4,72,8,512]{3,2,0,1:T(8,128)(2,1)S(1)}, bf16[4,72,8,512]{3,2,0,1:T(8,128)(2,1)}, u32[]{:S(2)}) copy-start(bf16[4,72,8,512]{3,2,0,1:T(8,128)(2,1)} %copy-done.2) | copy-start | bytes 7077892
  107.7 0.7 copy-start.7
  107.7 1.6 copy-start.4
  107.7 69.0 %reduce-scatter.3.cloned.1.call-start = ((), (), s32[]{:S(2)}) async-start(), calls=%async_computation.5 | async-start | bytes 2621440 | tf_op jit(solution)/shard_map/reduce_scatter | solution.py:119
  108.4 1.4 copy-start.10
  109.8 2.8 %copy-start.12 = (bf16[256]{0:T(256)(128)(2,1)S(1)}, bf16[256]{0:T(256)(128)(2,1)}, u32[]{:S(2)}) copy-start(bf16[256]{0:T(256)(128)(2,1)} %param.17) | copy-start | bytes 1540
  109.8 5.9 %copy-start.11 = (bf16[1,256,256]{2,1,0:T(8,128)(2,1)S(1)}, bf16[1,256,256]{2,1,0:T(8,128)(2,1)}, u32[]{:S(2)}) copy-start(bf16[1,256,256]{2,1,0:T(8,128)(2,1)} %param.16) | copy-start | bytes 393220
  110.6 5.0 %collective-permute-start = (bf16[15,256]{1,0:T(8,128)(2,1)S(1)}, bf16[15,256]{1,0:T(8,128)(2,1)S(1)}, u32[]{:S(2)}, u32[]{:S(2)}) collective-permute-start(bf16[15,256]{1,0:T(8,128)(2,1)S(1)} %slice.78), channel_id=1, source_target_pairs={{0,4},{4,8},{8,12},{12,16},{16,20},{20,24},{24,28},{28,32},{32,36}... | collective-permute-start | bytes 23048 | tf_op jit(solution)/shard_map/ppermute | solution.py:12
  119.2 30.7 %copy-start.6 = (f32[256,2]{0,1:T(2,128)S(1)}, f32[256,2]{0,1:T(2,128)}, u32[]{:S(2)}) copy-start(f32[256,2]{0,1:T(2,128)} %param.22) | copy-start | bytes 6148
  139.7 32.5 %all-to-all-start.2 = ((bf16[32,18,512]{2,1,0:T(8,128)(2,1)}), bf16[32,18,512]{2,1,0:T(8,128)(2,1)S(1)}, u32[]{:S(2)}, u32[]{:S(2)}) async-start(bf16[32,18,512]{2,1,0:T(8,128)(2,1)} %reshape.107), calls=%async_computation.4 | async-start | bytes 1572864 | tf_op jit(solution)/shard_map/all_to_all | solution.py:126
Sparse Core Ops, SparseCore 0:
  107.8 29.7 reduce-scatter.4
  140.7 32.0 reduce-scatter.2
